TPU v7x, 512 devices: a whole 4x4x16 slice. The times are simulated.
512 devices in a mesh: ep: 128 (over z, x, core), tp: 4 (over y).
Axes of the slice: x: 4, y: 4, z: 16, core: 2. Of those that a mesh axis runs over, the one named last changes fastest.
Arguments:
- tokens: bfloat16 [16384, 2048], P('ep'), may hold values from -6 to 6
- norm_gain: float32 [2048], replicated, may hold values from 0.1 to 1.9
- expert_ids: int32 [16384, 2], P('ep'), may hold values from 0 to 31, all different within a row; in each aligned block of 128 rows (0 to 127, 128 to 255, ...) at most 12 rows name the same one
- gate_weights: float32 [16384, 2], P('ep'), may hold values from 0.2 to 1
- w_gate: bfloat16 [2048, 131072], P(None, ('ep', 'tp')), may hold values from -0.125 to 0.125
- w_up: bfloat16 [2048, 131072], P(None, ('ep', 'tp')), may hold values from -0.125 to 0.125
- w_down: bfloat16 [131072, 2048], P('ep', 'tp'), may hold values from -0.09375 to 0.09375
Outputs:
- moe_out: bfloat16 [16384, 2048], P('ep', 'tp')
Inputs may be any that keep to these rules, and one draw needn't show every extreme that they name: `expert_ids`: each token names 2 different experts; in each aligned block of 128 rows no expert is named by more than 12 rows, a bound that some block reaches.
All inputs are finite; a program needn't handle non-finite values.
Results may differ from a plain program's by a relative error of at most 0.0071.
Values may be sent and summed in bfloat16 or wider, within the bound.
No kernel may reach another device: no remote copies, remote signals or barrier semaphores. Data moves between devices by JAX's collectives and lax.ppermute only.
A program may use at most 64 MiB of HBM per device.

v0:
```python
import jax
import jax.numpy as jnp
from jax import lax
from jax.sharding import Mesh
from jax.sharding import PartitionSpec as P

TOP = 2
EP = ("ep_0", "ep_1", "ep_2")
EP_TP = ("ep_0", "ep_1", "ep_2", "tp")
EPS = 1e-06


def split_up(array, dim, length):
    lengths = array.shape
    parts = array.reshape(*lengths[:dim], length, lengths[dim] // length, *lengths[dim + 1 :])
    return jnp.moveaxis(parts, dim, 0)


def laid_out(parts, dim):
    parts = jnp.moveaxis(parts, 0, dim)
    lengths = parts.shape
    return parts.reshape(*lengths[:dim], lengths[dim] * lengths[dim + 1], *lengths[dim + 2 :])


def turned_blocks(parts, axes, sequence):
    inside = parts.shape[1:]
    out = parts.reshape(*(lax.axis_size(a) for a in axes), *inside)
    for k in sequence:
        out = lax.all_to_all(out, axes[k], k, k, tiled=True)
    return out.reshape(-1, *inside)


def exchange_by_chip(array, groups, sequence, split_dim, concat_dim):
    length = lax.axis_size(groups[0]) * lax.axis_size(groups[1])
    parts = split_up(array, split_dim, length)
    return laid_out(turned_blocks(parts, groups, sequence), concat_dim)


def rms_rows(values, gain):
    widened = values.astype(jnp.float32)
    scale = lax.rsqrt(jnp.mean(widened * widened, axis=-1, keepdims=True) + EPS)
    return (widened * scale * gain).astype(jnp.bfloat16)


def on_device(tokens, norm_gain, expert_ids, gate_weights, w_gate, w_up, w_down):
    ep_count = lax.axis_size(EP)
    tp_count = lax.axis_size("tp")
    row_count = tokens.shape[0]
    group_size = max(1, ep_count // 32)
    expert_count = ep_count // group_size
    share = (row_count * TOP * 5 + 4 * expert_count * tp_count - 1) // (4 * expert_count * tp_count)
    capacity = min(row_count, tp_count * share)
    normed = rms_rows(tokens, norm_gain)
    flat_ids = expert_ids.reshape(-1)
    matches = (flat_ids[:, None] == jnp.arange(expert_count, dtype=jnp.int32)[None, :]).astype(
        jnp.int32
    )
    slot_index = jnp.sum((jnp.cumsum(matches, axis=0) - matches) * matches, axis=1)
    position = flat_ids * capacity + slot_index
    placing = (
        position[:, None] == jnp.arange(expert_count * capacity, dtype=jnp.int32)[None, :]
    ).astype(jnp.float32)
    placing = placing.reshape(row_count, TOP, expert_count * capacity)
    selector = jnp.sum(placing, axis=1).astype(jnp.bfloat16)
    buffers = lax.dot_general(
        selector, normed, (((0,), (0,)), ((), ())), preferred_element_type=jnp.float32
    )
    buffers = buffers.astype(jnp.bfloat16).reshape(expert_count, capacity, -1)
    quarter = capacity // tp_count
    mine = lax.dynamic_slice_in_dim(buffers, lax.axis_index("tp") * quarter, quarter, 1)
    copies = jnp.repeat(mine, group_size, axis=0)
    arrived = exchange_by_chip(copies, (("ep_0", "ep_1"), "ep_2"), (1, 0), 0, 0)
    received = lax.all_gather(arrived, "tp", axis=1, tiled=True)
    sources, slot_count, model_width = received.shape
    flat_rows = received.reshape(sources * slot_count, model_width)
    gate_proj = jnp.dot(flat_rows, w_gate, preferred_element_type=jnp.float32)
    upper = jnp.dot(flat_rows, w_up, preferred_element_type=jnp.float32)
    hidden = (jax.nn.silu(gate_proj) * upper).astype(jnp.bfloat16)
    partial_out = jnp.dot(
        lax.all_gather(hidden, "tp", axis=1, tiled=True), w_down, preferred_element_type=jnp.float32
    ).astype(jnp.bfloat16)
    partial_out = partial_out.reshape(sources, slot_count, w_down.shape[1])
    sources, slot_count, out_width = partial_out.shape
    back = exchange_by_chip(partial_out, (("ep_0", "ep_1"), "ep_2"), (1, 0), 0, 0)
    back = back.reshape(expert_count, group_size, slot_count, out_width).astype(jnp.float32)
    returned = jnp.sum(back, axis=1)
    summed = returned.reshape(expert_count * capacity, -1)
    combine = jnp.sum(placing * gate_weights[:, :, None], axis=1)
    mixed = jnp.dot(
        combine, summed, precision=lax.Precision.HIGHEST, preferred_element_type=jnp.float32
    )
    return mixed.astype(jnp.bfloat16)


def solution(mesh):
    finer = Mesh(mesh.devices.reshape(16, 4, 2, mesh.shape["tp"]), ("ep_0", "ep_1", "ep_2", "tp"))
    placed = (
        P(EP, None),
        P(),
        P(EP, None),
        P(EP, None),
        P(None, EP_TP),
        P(None, EP_TP),
        P(EP, "tp"),
    )
    return jax.shard_map(
        on_device, mesh=finer, in_specs=placed, out_specs=P(EP, "tp"), check_vma=False
    )
```

profile of v0, /device:TPU:2, one launch (start us, length us, event | category | flops | bytes accessed | tf_op | source)
XLA Modules:
  0.0 389.9 jit_solution(7729169001689056819)
XLA Ops:
  6.5 0.9 copy.81
  7.7 1.2 fusion.1
  9.0 0.6 reduce-window.6
  10.1 0.7 multiply_add_fusion
  10.8 0.8 convert_reduce_fusion.1
  11.7 1.4 convolution_convert_fusion.1
  13.1 1.5 reshape.57
  14.6 2.0 constant_dynamic-slice_fusion
  16.6 0.3 copy.85
  16.9 0.5 broadcast_in_dim.6
  17.4 0.3 broadcast_in_dim.14
  17.8 5.0 %all_to_all.20 = bf16[64,2,1,3,2048]{4,0,3,2,1:T(8,128)(2,1)S(1)} all-to-all(bf16[64,2,1,3,2048]{4,0,3,2,1:T(8,128)(2,1)S(1)} %broadcast_in_dim.15), channel_id=1, replica_groups=mesh['ep_0'=16,'ep_1'=4,'ep_2'=2,'tp'=4] {'ep_2'}, dimensions={1} | all-to-all | bytes 3145728 | tf_op jit(solution)/shard_map/all_to_all | solution.py:29
  22.8 1.6 copy.86
  24.5 96.4 %all_to_all.21 = bf16[64,2,1,3,2048]{4,1,3,2,0:T(2,128)(2,1)S(1)} all-to-all(bf16[64,2,1,3,2048]{4,1,3,2,0:T(2,128)(2,1)S(1)} %copy.86), channel_id=1, replica_groups=mesh['ep_0'=16,'ep_1'=4,'ep_2'=2,'tp'=4] {'ep_0','ep_1'}, dimensions={0} | all-to-all | bytes 3145728 | tf_op jit(solution)/shard_map/all_to_all | solution.py:29
  120.8 1.1 copy.87
  122.0 2.0 reshape_reshape.3
  124.0 0.2 all-gather.5.cloned.1.call-start
  124.3 65.0 %all-gather.3.cloned.1.call-done = bf16[128,12,2048]{2,0,1:T(8,128)(2,1)} async-done(((bf16[128,3,2048]{2,0,1:T(8,128)(2,1)}), bf16[128,12,2048]{2,0,1:T(8,128)(2,1)}) %all-gather.3.cloned.1.call-update) | async-done | bytes 6291472 | tf_op jit(solution)/shard_map/all_gather | solution.py:73
  189.3 9.7 %copy.88 = bf16[128,12,2048]{2,1,0:T(8,128)(2,1)} copy(bf16[128,12,2048]{2,0,1:T(8,128)(2,1)} %all-gather.3.cloned.1.call-done) | data formatting | bytes 12582912 | tf_op jit(solution)/shard_map/all_gather | solution.py:73
  198.9 10.8 %reshape.58 = bf16[1536,2048]{1,0:T(8,128)(2,1)} reshape(bf16[128,12,2048]{2,1,0:T(8,128)(2,1)} %copy.88) | data formatting | bytes 12582912 | tf_op jit(solution)/shard_map/reshape | solution.py:75
  209.7 4.8 %fusion.12 = f32[1536,256]{1,0:T(8,128)S(1)} fusion(bf16[1536,2048]{1,0:T(8,128)(2,1)} %reshape.58, bf16[2048,256]{1,0:T(8,128)(2,1)S(1)} %copy-done.3), kind=kOutput, calls=%fused_computation.30 | convolution fusion | flops 1610612736 | bytes 8912896 | tf_op jit(solution)/shard_map/dot_general | solution.py:76
  214.6 3.0 fusion
  217.6 51.2 %all-gather.5.cloned.1.call-done = bf16[1536,1024]{1,0:T(8,128)(2,1)} async-done(((bf16[1536,256]{1,0:T(8,128)(2,1)}), bf16[1536,1024]{1,0:T(8,128)(2,1)}) %all-gather.5.cloned.1.call-update) | async-done | bytes 3145744 | tf_op jit(solution)/shard_map/all_gather | solution.py:80
  268.8 4.8 %convolution_convert_fusion = bf16[1536,512]{1,0:T(8,128)(2,1)} fusion(bf16[1536,1024]{1,0:T(8,128)(2,1)} %all-gather.5.cloned.1.call-done, bf16[1024,512]{1,0:T(8,128)(2,1)S(1)} %copy-done), kind=kOutput, calls=%fused_computation.1 | convolution fusion | flops 1611399168 | bytes 5767168 | tf_op jit(solution)/shard_map/dot_general | solution.py:79
  273.6 2.4 reshape_reshape_reshape.2
  276.0 0.9 copy.89
  276.8 5.0 %all_to_all.22 = bf16[64,2,1,12,512]{4,0,3,2,1:T(8,128)(2,1)S(1)} all-to-all(bf16[64,2,1,12,512]{4,0,3,2,1:T(8,128)(2,1)S(1)} %copy.89), channel_id=1, replica_groups=mesh['ep_0'=16,'ep_1'=4,'ep_2'=2,'tp'=4] {'ep_2'}, dimensions={1} | all-to-all | bytes 3145728 | tf_op jit(solution)/shard_map/all_to_all | solution.py:29
  281.8 1.6 copy.90
  283.5 93.7 %all_to_all.23 = bf16[64,2,1,12,512]{4,1,3,2,0:T(2,128)(2,1)S(1)} all-to-all(bf16[64,2,1,12,512]{4,1,3,2,0:T(2,128)(2,1)S(1)} %copy.90), channel_id=1, replica_groups=mesh['ep_0'=16,'ep_1'=4,'ep_2'=2,'tp'=4] {'ep_0','ep_1'}, dimensions={0} | all-to-all | bytes 3145728 | tf_op jit(solution)/shard_map/all_to_all | solution.py:29
  377.1 4.2 %convert_reduce_fusion = f32[64,12,512]{2,1,0:T(8,128)S(1)} fusion(bf16[64,2,1,12,512]{4,1,3,2,0:T(2,128)(2,1)S(1)} %all_to_all.23), kind=kLoop, calls=%fused_computation | loop fusion | flops 1179648 | bytes 3145728 | tf_op jit(solution)/shard_map/reduce_sum | solution.py:86
  381.4 0.3 bitcast_reduce_fusion
  381.7 1.3 convolution_convert_fusion.2
  (25 shorter events, 1.2 us)
Async XLA Ops:
  6.5 262.3 %copy-start = (bf16[1024,512]{1,0:T(8,128)(2,1)S(1)}, bf16[1024,512]{1,0:T(8,128)(2,1)}, u32[]{:S(2)}) copy-start(bf16[1024,512]{1,0:T(8,128)(2,1)} %param.13) | copy-start | bytes 3145732
  6.5 5.1 %copy-start.2 = (bf16[128,2048]{1,0:T(8,128)(2,1)S(1)}, bf16[128,2048]{1,0:T(8,128)(2,1)}, u32[]{:S(2)}) copy-start(bf16[128,2048]{1,0:T(8,128)(2,1)} %param.7) | copy-start | bytes 1572868
  6.5 182.7 %all-gather.3.cloned.1.call-start = ((), (), s32[]{:S(2)}) async-start(), calls=%async_computation.4 | async-start | bytes 7864320 | tf_op jit(solution)/shard_map/all_gather | solution.py:73
  124.0 144.7 %all-gather.5.cloned.1.call-start = ((), (), s32[]{:S(2)}) async-start(), calls=%async_computation.5 | async-start | bytes 3932160 | tf_op jit(solution)/shard_map/all_gather | solution.py:80
  198.9 10.8 %copy-start.3 = (bf16[2048,256]{1,0:T(8,128)(2,1)S(1)}, bf16[2048,256]{1,0:T(8,128)(2,1)}, u32[]{:S(2)}) copy-start(bf16[2048,256]{1,0:T(8,128)(2,1)} %param.11) | copy-start | bytes 3145732
  209.7 4.8 %copy-start.1 = (bf16[1536,2048]{1,0:T(8,128)(2,1)S(1)}, bf16[1536,2048]{1,0:T(8,128)(2,1)}, u32[]{:S(2)}) copy-start(bf16[1536,2048]{1,0:T(8,128)(2,1)} %reshape.58) | copy-start | bytes 18874372
  209.7 4.9 %copy-start.4 = (bf16[2048,256]{1,0:T(8,128)(2,1)S(1)}, bf16[2048,256]{1,0:T(8,128)(2,1)}, u32[]{:S(2)}) copy-start(bf16[2048,256]{1,0:T(8,128)(2,1)} %param.12) | copy-start | bytes 3145732
Sparse Core Ops, SparseCore 0:
  124.2 65.0 all-gather.2
  217.7 51.0 all-gather.4
where the time goes:
time: 391 us; the launch traced here: 390 us
  blocking collectives  200 us (51%)
  waiting for transfers between devices  116 us (30%)
  local copies, waits for them, and re-layouts  36.5 us (9%)
  matrix products  15.2 us (4%)
  between operations  13.6 us (3%)
  other arithmetic  8.01 us (2%)
    all_to_all x4, blocking collectives, turned_blocks(): out = lax.all_to_all(out, axes[k], k, k, tiled=True)  200 us
    all_gather x1, waiting for transfers between devices, on_device(): received = lax.all_gather(arrived, 'tp', axis=1, tiled=True)  65 us
    all_gather x1, waiting for transfers between devices, on_device(): lax.all_gather(hidden, 'tp', axis=1, tiled=True)  51.2 us
    reshape x1, local copies, waits for them, and re-layouts, on_device(): flat_rows = received.reshape(sources * slot_count, model_width)  10.8 us
    all_gather x1, local copies, waits for them, and re-layouts, on_device(): received = lax.all_gather(arrived, 'tp', axis=1, tiled=True)  9.65 us
  transfers between devices with their start and end apart: 2, of which 2 were waited for; matrix products, arithmetic and copies ran while one was open for 0% of the time, Pallas kernels for 0%

commit v1 on v0

--- a/solution.py
+++ b/solution.py
@@ -8,6 +8,11 @@
 EP = ("ep_0", "ep_1", "ep_2")
 EP_TP = ("ep_0", "ep_1", "ep_2", "tp")
 EPS = 1e-06
+
+
+def all_by_exchange(x, axis, along):
+    repeated = jnp.stack([x] * lax.axis_size(axis))
+    return jnp.concatenate(lax.all_to_all(repeated, axis, 0, 0), axis=along)
 
 
 def split_up(array, dim, length):
@@ -77,7 +82,7 @@
     upper = jnp.dot(flat_rows, w_up, preferred_element_type=jnp.float32)
     hidden = (jax.nn.silu(gate_proj) * upper).astype(jnp.bfloat16)
     partial_out = jnp.dot(
-        lax.all_gather(hidden, "tp", axis=1, tiled=True), w_down, preferred_element_type=jnp.float32
+        all_by_exchange(hidden, "tp", 1), w_down, preferred_element_type=jnp.float32
     ).astype(jnp.bfloat16)
     partial_out = partial_out.reshape(sources, slot_count, w_down.shape[1])
     sources, slot_count, out_width = partial_out.shape

time: 391 us -> 378 us (0.967)
  waiting for transfers between devices: 116 us -> 65.3 us
  blocking collectives: 200 us -> 241 us
    all_gather x1 -> x0, waiting for transfers between devices: 51.2 us -> none  [on_device(): lax.all_gather(hidden, 'tp', axis=1, tiled=True)]
    all_to_all x0 -> x1, blocking collectives: none -> 40.9 us  [all_by_exchange(): return jnp.concatenate(lax.all_to_all(repeated, axis, 0, 0), axis=along)]
  transfers between devices with their start and end apart: 2 -> 1, of which waited for: 2 -> 1; matrix products, arithmetic and copies ran while one was open for 0% -> 0% of each run, Pallas kernels for 0% -> 0%
where the time goes in v1:
time: 378 us; the launch traced here: 377 us
  blocking collectives  241 us (64%)
  waiting for transfers between devices  65.3 us (17%)
  local copies, waits for them, and re-layouts  37 us (10%)
  between operations  13.6 us (4%)
  matrix products  12.5 us (3%)
  other arithmetic  8.01 us (2%)
    all_to_all x4, blocking collectives, turned_blocks(): out = lax.all_to_all(out, axes[k], k, k, tiled=True)  200 us
    all_gather x1, waiting for transfers between devices, on_device(): received = lax.all_gather(arrived, 'tp', axis=1, tiled=True)  65.3 us
    all_to_all x1, blocking collectives, all_by_exchange(): return jnp.concatenate(lax.all_to_all(repeated, axis, 0, 0), axis=along)  40.9 us
    reshape x1, local copies, waits for them, and re-layouts, on_device(): flat_rows = received.reshape(sources * slot_count, model_width)  10.8 us
    all_gather x1, local copies, waits for them, and re-layouts, on_device(): received = lax.all_gather(arrived, 'tp', axis=1, tiled=True)  9.65 us
  transfers between devices with their start and end apart: 1, of which 1 were waited for; matrix products, arithmetic and copies ran while one was open for 0% of the time, Pallas kernels for 0%

profile of v1, /device:TPU:2, one launch (start us, length us, event | category | flops | bytes accessed | tf_op | source)
XLA Modules:
  0.0 377.1 jit_solution(13730696275977817900)
XLA Ops:
  6.5 0.9 copy.87
  7.7 1.2 fusion.1
  9.0 0.6 reduce-window.6
  10.1 0.7 multiply_add_fusion
  10.8 0.8 convert_reduce_fusion.1
  11.7 1.4 convolution_convert_fusion.1
  13.1 1.5 reshape.65
  14.6 2.0 constant_dynamic-slice_fusion
  16.6 0.3 copy.91
  16.9 0.5 broadcast_in_dim.6
  17.4 0.3 broadcast_in_dim.14
  17.8 5.0 %all_to_all.25 = bf16[64,2,1,3,2048]{4,0,3,2,1:T(8,128)(2,1)S(1)} all-to-all(bf16[64,2,1,3,2048]{4,0,3,2,1:T(8,128)(2,1)S(1)} %broadcast_in_dim.15), channel_id=1, replica_groups=mesh['ep_0'=16,'ep_1'=4,'ep_2'=2,'tp'=4] {'ep_2'}, dimensions={1} | all-to-all | bytes 3145728 | tf_op jit(solution)/shard_map/all_to_all | solution.py:34
  22.8 1.6 copy.92
  24.5 96.4 %all_to_all.26 = bf16[64,2,1,3,2048]{4,1,3,2,0:T(2,128)(2,1)S(1)} all-to-all(bf16[64,2,1,3,2048]{4,1,3,2,0:T(2,128)(2,1)S(1)} %copy.92), channel_id=1, replica_groups=mesh['ep_0'=16,'ep_1'=4,'ep_2'=2,'tp'=4] {'ep_0','ep_1'}, dimensions={0} | all-to-all | bytes 3145728 | tf_op jit(solution)/shard_map/all_to_all | solution.py:34
  120.8 1.1 copy.93
  122.0 2.0 reshape_reshape.3
  124.0 65.3 %all-gather.2.cloned.1.call-done = bf16[128,12,2048]{2,0,1:T(8,128)(2,1)} async-done(((bf16[128,3,2048]{2,0,1:T(8,128)(2,1)}), bf16[128,12,2048]{2,0,1:T(8,128)(2,1)}) %all-gather.2.cloned.1.call-update) | async-done | bytes 6291472 | tf_op jit(solution)/shard_map/all_gather | solution.py:78
  189.3 9.7 %copy.94 = bf16[128,12,2048]{2,1,0:T(8,128)(2,1)} copy(bf16[128,12,2048]{2,0,1:T(8,128)(2,1)} %all-gather.2.cloned.1.call-done) | data formatting | bytes 12582912 | tf_op jit(solution)/shard_map/all_gather | solution.py:78
  198.9 10.8 %reshape.66 = bf16[1536,2048]{1,0:T(8,128)(2,1)} reshape(bf16[128,12,2048]{2,1,0:T(8,128)(2,1)} %copy.94) | data formatting | bytes 12582912 | tf_op jit(solution)/shard_map/reshape | solution.py:80
  209.7 4.8 %fusion.12 = f32[1536,256]{1,0:T(8,128)S(1)} fusion(bf16[1536,2048]{1,0:T(8,128)(2,1)} %reshape.66, bf16[2048,256]{1,0:T(8,128)(2,1)S(1)} %copy-done.3), kind=kOutput, calls=%fused_computation.30 | convolution fusion | flops 1610612736 | bytes 8912896 | tf_op jit(solution)/shard_map/dot_general | solution.py:81
  214.6 2.1 fusion
  216.7 0.3 copy.95
  217.2 40.9 %all_to_all.27 = bf16[4,1536,256]{1,2,0:T(8,128)(2,1)S(1)} all-to-all(bf16[4,1536,256]{1,2,0:T(8,128)(2,1)S(1)} %stack.2), channel_id=1, replica_groups=mesh['ep_0'=16,'ep_1'=4,'ep_2'=2,'tp'=4] {'tp'}, dimensions={0} | all-to-all | bytes 6291456 | tf_op jit(solution)/shard_map/all_to_all | solution.py:15
  258.1 3.0 convolution_convert_fusion
  261.0 2.4 reshape_reshape_reshape.2
  263.4 0.9 copy.96
  264.3 5.0 %all_to_all.28 = bf16[64,2,1,12,512]{4,0,3,2,1:T(8,128)(2,1)S(1)} all-to-all(bf16[64,2,1,12,512]{4,0,3,2,1:T(8,128)(2,1)S(1)} %copy.96), channel_id=1, replica_groups=mesh['ep_0'=16,'ep_1'=4,'ep_2'=2,'tp'=4] {'ep_2'}, dimensions={1} | all-to-all | bytes 3145728 | tf_op jit(solution)/shard_map/all_to_all | solution.py:34
  269.3 1.6 copy.97
  270.9 93.5 %all_to_all.29 = bf16[64,2,1,12,512]{4,1,3,2,0:T(2,128)(2,1)S(1)} all-to-all(bf16[64,2,1,12,512]{4,1,3,2,0:T(2,128)(2,1)S(1)} %copy.97), channel_id=1, replica_groups=mesh['ep_0'=16,'ep_1'=4,'ep_2'=2,'tp'=4] {'ep_0','ep_1'}, dimensions={0} | all-to-all | bytes 3145728 | tf_op jit(solution)/shard_map/all_to_all | solution.py:34
  364.4 4.2 %convert_reduce_fusion = f32[64,12,512]{2,1,0:T(8,128)S(1)} fusion(bf16[64,2,1,12,512]{4,1,3,2,0:T(2,128)(2,1)S(1)} %all_to_all.29), kind=kLoop, calls=%fused_computation | loop fusion | flops 1179648 | bytes 3145728 | tf_op jit(solution)/shard_map/reduce_sum | solution.py:91
  368.6 0.3 bitcast_reduce_fusion
  368.9 1.3 convolution_convert_fusion.2
  (25 shorter events, 1.4 us)
Async XLA Ops:
  6.5 251.5 %copy-start = (bf16[1024,512]{1,0:T(8,128)(2,1)S(1)}, bf16[1024,512]{1,0:T(8,128)(2,1)}, u32[]{:S(2)}) copy-start(bf16[1024,512]{1,0:T(8,128)(2,1)} %param.13) | copy-start | bytes 3145732
  6.5 5.1 %copy-start.2 = (bf16[128,2048]{1,0:T(8,128)(2,1)S(1)}, bf16[128,2048]{1,0:T(8,128)(2,1)}, u32[]{:S(2)}) copy-start(bf16[128,2048]{1,0:T(8,128)(2,1)} %param.7) | copy-start | bytes 1572868
  6.5 182.7 %all-gather.2.cloned.1.call-start = ((), (), s32[]{:S(2)}) async-start(), calls=%async_computation.5 | async-start | bytes 7864320 | tf_op jit(solution)/shard_map/all_gather | solution.py:78
  198.9 10.8 %copy-start.3 = (bf16[2048,256]{1,0:T(8,128)(2,1)S(1)}, bf16[2048,256]{1,0:T(8,128)(2,1)}, u32[]{:S(2)}) copy-start(bf16[2048,256]{1,0:T(8,128)(2,1)} %param.11) | copy-start | bytes 3145732
  209.7 4.8 %copy-start.1 = (bf16[1536,2048]{1,0:T(8,128)(2,1)S(1)}, bf16[1536,2048]{1,0:T(8,128)(2,1)}, u32[]{:S(2)}) copy-start(bf16[1536,2048]{1,0:T(8,128)(2,1)} %reshape.66) | copy-start | bytes 18874372
  209.7 4.9 %copy-start.4 = (bf16[2048,256]{1,0:T(8,128)(2,1)S(1)}, bf16[2048,256]{1,0:T(8,128)(2,1)}, u32[]{:S(2)}) copy-start(bf16[2048,256]{1,0:T(8,128)(2,1)} %param.12) | copy-start | bytes 3145732
Sparse Core Ops, SparseCore 0:
  124.2 65.0 all-gather.1
